TPU v7x, 32 devices: a whole 2x2x4 slice. The times are simulated.
32 devices in a mesh: ep: 8 (over z, x), tp: 4 (over y, core).
Axes of the slice: x: 2, y: 2, z: 4, core: 2. Of those that a mesh axis runs over, the one named last changes fastest.
Arguments:
- tokens: bfloat16 [1024, 4096], P('ep', 'tp'), may hold values from -6 to 6
- cotangent: bfloat16 [1024, 4096], P('ep', 'tp'), may hold values from -6 to 6
- routes: int32 [1024, 2], P('ep'), may hold values from 0 to 7, all different within a row; in each aligned block of 128 rows (0 to 127, 128 to 255, ...) at most 48 rows name the same one
- gate_weight: float32 [1024, 2], P('ep'), may hold values from 0.1 to 2.5
- w_gate: bfloat16 [8, 1024, 4096], P('ep', 'tp'), may hold values from -0.09375 to 0.09375
- w_up: bfloat16 [8, 1024, 4096], P('ep', 'tp'), may hold values from -0.09375 to 0.09375
- w_down: bfloat16 [8, 1024, 4096], P('ep', 'tp'), may hold values from -0.1875 to 0.1875
- shared_hidden: bfloat16 [1024, 1024], P('ep'), may hold values from -4 to 4
Outputs:
- tokens_grad: bfloat16 [1024, 4096], P('ep', 'tp')
- gate_grad: float32 [1024, 2], P('ep')
- w_gate_grad: float32 [8, 1024, 4096], P('ep', 'tp')
- w_up_grad: float32 [8, 1024, 4096], P('ep', 'tp')
- w_down_grad: float32 [8, 1024, 4096], P('ep', 'tp')
- shared_grad: float32 [1024, 4096], P('ep', 'tp')
Inputs may be any that keep to these rules, and one draw needn't show every extreme that they name: `routes`: each row names 2 different experts. Among the rows of one index of ep (aligned blocks of 128 rows) no expert is named more than 48 times, and in every draw some expert is named exactly 48 times in some block.
All inputs are finite; a program needn't handle non-finite values.
Results may differ from a plain program's by a relative error of at most 0.022.
Values may be sent and summed in bfloat16 or wider, within the bound.
A program may use at most 64 MiB of HBM per device.

v0:
```python
import functools

import jax
import jax.numpy as jnp
from jax import lax
from jax.experimental import pallas as pl
from jax.experimental.pallas import tpu as pltpu
from jax.sharding import PartitionSpec as P

MESH = pl.DeviceIdType.MESH
BF16 = jnp.bfloat16
F32 = jnp.float32


def dispatch_kernel(
    dims,
    tok_ref,
    meta_ref,
    cot_ref,
    sh_ref,
    xfull,
    gfull,
    meta_out,
    cot_all,
    sh_out,
    local_sem,
    meta_send,
    meta_recv,
    tok_send,
    tok_recv,
    sh_send,
    sh_recv,
    cot_up,
    cot_down,
    cot_side,
    cot_recv,
    y_send,
    y_recv,
    sib_send,
    sib_recv,
):
    E, T, X, C, F, N = dims
    Y = T // 2
    NZ = E // X
    me = lax.axis_index("ep")
    tp = lax.axis_index("tp")
    y = tp // 2
    c = tp % 2
    sib = y * 2 + (1 - c)
    z = me // X
    x = me % X
    full = (xfull, gfull)

    barrier = pltpu.get_barrier_semaphore()

    def greet(d, _):
        pl.semaphore_signal(
            barrier, inc=1, device_id=((me + d) % E, tp), device_id_type=MESH
        )
        return 0

    lax.fori_loop(1, E, greet, 0)
    for dt in range(1, T):
        pl.semaphore_signal(
            barrier, inc=1, device_id=(me, (tp + dt) % T), device_id_type=MESH
        )
    pl.semaphore_wait(barrier, (E - 1) + (T - 1))

    def rows_of(s):
        return pl.ds(pl.multiple_of(s * C, 16), C)

    def cols_of(t):
        return pl.ds(pl.multiple_of(t * F, 128), F)

    def lanes_of(s):
        return pl.ds(pl.multiple_of(s * N, 128), N)

    def remote(src, dst, ss, rs, dev):
        return pltpu.make_async_remote_copy(
            src_ref=src,
            dst_ref=dst,
            send_sem=ss,
            recv_sem=rs,
            device_id=dev,
            device_id_type=MESH,
        )

    def meta_copy(dst):
        return remote(
            meta_ref.at[dst], meta_out.at[me], meta_send.at[dst], meta_recv.at[me], (dst, tp)
        )

    def tok_copy(dst):
        return remote(
            tok_ref.at[dst],
            xfull.at[rows_of(me), cols_of(tp)],
            tok_send.at[dst],
            tok_recv.at[me],
            (dst, tp),
        )

    def sh_copy(dst):
        return remote(
            sh_ref.at[dst], sh_out.at[:, lanes_of(me)], sh_send.at[dst], sh_recv.at[me], (dst, tp)
        )

    def cot_copy(s, sems, dst):
        return remote(cot_all.at[s], cot_all.at[s], sems.at[s], cot_recv.at[s], (dst, tp))

    locals_ = (
        pltpu.make_async_copy(cot_ref, cot_all.at[me], local_sem.at[0]),
        pltpu.make_async_copy(
            tok_ref.at[me], xfull.at[rows_of(me), cols_of(tp)], local_sem.at[1]
        ),
        pltpu.make_async_copy(meta_ref.at[me], meta_out.at[me], local_sem.at[2]),
        pltpu.make_async_copy(sh_ref.at[me], sh_out.at[:, lanes_of(me)], local_sem.at[3]),
    )
    for cp in locals_:
        cp.start()
    for cp in locals_:
        cp.wait()

    def each_source(fn, first=0):
        def step(i, _):
            k = i // X
            dz = ((k + 1) // 2) * (1 - 2 * (k % 2))
            zs = z + dz
            dx = i % X

            @pl.when((zs >= 0) & (zs < NZ))
            def _():
                fn(i, dz, dx, zs * X + (x + dx) % X)

            return 0

        lax.fori_loop(first, (2 * NZ - 1) * X, step, 0)

    def spread_cot(dz, s, act):
        @pl.when((dz <= 0) & (z + 1 < NZ))
        def _():
            act(cot_copy(s, cot_up, me + X))

        @pl.when((dz >= 0) & (z >= 1))
        def _():
            act(cot_copy(s, cot_down, me - X))

        for d in range(1, X):
            act(cot_copy(s, cot_side.at[d - 1], z * X + (x + d) % X))

    def start(cp):
        cp.start()

    def wait_send(cp):
        cp.wait_send()

    spread_cot(me * 0, me, start)

    def send_small(i, dz, dx, s):
        meta_copy(s).start()

    def send_rows(i, dz, dx, s):
        tok_copy(s).start()

    each_source(send_small, 1)
    each_source(send_rows, 1)

    def y_copy(a, s, dy):
        part = full[a].at[rows_of(s), cols_of(tp)]
        return remote(
            part,
            part,
            y_send.at[a, dy - 1],
            y_recv.at[a, dy - 1, s],
            (me, ((y + dy) % Y) * 2 + c),
        )

    def sib_copy(a, s, dy):
        part = full[a].at[rows_of(s), cols_of(((y + Y - dy) % Y) * 2 + c)]
        return remote(part, part, sib_send.at[a, dy], sib_recv.at[a, dy], (me, sib))

    def forward(a, s):
        for dy in range(1, Y):
            y_copy(a, s, dy).start()
        sib_copy(a, s, 0).start()

    def take_rows(i, dz, dx, s):
        @pl.when(s != me)
        def _():
            remote(
                tok_ref.at[s],
                xfull.at[rows_of(s), cols_of(tp)],
                tok_send.at[s],
                tok_recv.at[s],
                (me, tp),
            ).wait_recv()

        forward(0, s)

    def take_cot(i, dz, dx, s):
        @pl.when(s != me)
        def _():
            remote(
                cot_all.at[s], cot_all.at[s], cot_up.at[s], cot_recv.at[s], (me, tp)
            ).wait_recv()

            @pl.when(dx == 0)
            def _():
                spread_cot(dz, s, start)

            remote(
                meta_ref.at[s], meta_out.at[s], meta_send.at[s], meta_recv.at[s], (me, tp)
            ).wait_recv()

        picked = jnp.dot(
            meta_out[s, :, :N], cot_all[s], preferred_element_type=F32
        ).astype(BF16)
        gfull[rows_of(s), cols_of(tp)] = picked
        forward(1, s)

        @pl.when(s != me)
        def _():
            sh_copy(s).start()

    def relay(a, s):
        for dy in range(1, Y):
            part = full[a].at[rows_of(s), cols_of(((y + Y - dy) % Y) * 2 + c)]
            remote(
                part, part, y_send.at[a, dy - 1], y_recv.at[a, dy - 1, s], (me, tp)
            ).wait_recv()
            sib_copy(a, s, dy).start()

    def relay_rows(i, dz, dx, s):
        relay(0, s)

    def relay_cot(i, dz, dx, s):
        relay(1, s)

    def guarded(fn, j):
        k = j // X
        dz = ((k + 1) // 2) * (1 - 2 * (k % 2))
        zs = z + dz
        dx = j % X

        @pl.when((j >= 0) & (zs >= 0) & (zs < NZ))
        def _():
            fn(j, dz, dx, zs * X + (x + dx) % X)

    total = (2 * NZ - 1) * X

    def main(i, _):
        guarded(take_rows, i)
        guarded(take_cot, i - X)
        guarded(relay_rows, i - X)
        guarded(relay_cot, i - 2 * X)
        return 0

    lax.fori_loop(0, total + 2 * X, main, 0)

    def finish(i, dz, dx, s):
        @pl.when(s != me)
        def _():
            meta_copy(s).wait_send()
            tok_copy(s).wait_send()
            sh_copy(s).wait_send()
            remote(
                sh_ref.at[s], sh_out.at[:, lanes_of(s)], sh_send.at[s], sh_recv.at[s], (me, tp)
            ).wait_recv()

        @pl.when(dx == 0)
        def _():
            spread_cot(dz, s, wait_send)

    each_source(finish)
    for a in (0, 1):
        mine = full[a].at[:, cols_of(tp)]
        for dy in range(1, Y):
            remote(mine, mine, y_send.at[a, dy - 1], y_send.at[a, dy - 1], (me, sib)).wait_send()
        for dy in range(Y):
            other = full[a].at[:, cols_of(((y + Y - dy) % Y) * 2 + 1 - c)]
            cp = remote(other, other, sib_send.at[a, dy], sib_recv.at[a, dy], (me, sib))
            cp.wait_send()
            cp.wait_recv()


def return_kernel(
    dims,
    part,
    gate,
    back,
    gate_back,
    pair_in,
    y_out,
    y_in,
    row_out,
    gate_in,
    gate_out,
    pair_send,
    pair_recv,
    y_send,
    y_recv,
    back_send,
    back_recv,
    gate_tp_send,
    gate_tp_recv,
    gate_ep_send,
    gate_ep_recv,
):
    E, T, C, F = dims
    Y = T // 2
    me = lax.axis_index("ep")
    tp = lax.axis_index("tp")
    y = tp // 2
    c = tp % 2
    sib = y * 2 + (1 - c)

    def rows_of(s):
        return pl.ds(pl.multiple_of(s * C, 16), C)

    def cols_of(t):
        return pl.ds(pl.multiple_of(t * F, 128), F)

    def remote(src, dst, ss, rs, dev):
        return pltpu.make_async_remote_copy(
            src_ref=src,
            dst_ref=dst,
            send_sem=ss,
            recv_sem=rs,
            device_id=dev,
            device_id_type=MESH,
        )

    def source(i):
        return (me + E // 2 + i) % E

    def pair_copy(s, dy):
        return remote(
            part.at[rows_of(s), cols_of(((y + dy) % Y) * 2 + 1 - c)],
            pair_in.at[dy, rows_of(s)],
            pair_send.at[dy],
            pair_recv.at[dy, s],
            (me, sib),
        )

    def gate_tp_copy(dt):
        return remote(
            gate, gate_in.at[dt], gate_tp_send.at[dt], gate_tp_recv.at[dt], (me, (tp + dt) % T)
        )

    def gate_ep_copy(s):
        return remote(gate_out.at[s], gate_back.at[me], gate_ep_send, gate_ep_recv, (s, tp))

    def y_copy(s, dy):
        return remote(
            y_out.at[dy - 1, rows_of(s)],
            y_in.at[dy - 1, rows_of(s)],
            y_send.at[dy - 1],
            y_recv.at[dy - 1, s],
            (me, ((y + dy) % Y) * 2 + c),
        )

    def back_copy(s):
        return remote(row_out.at[rows_of(s)], back.at[me], back_send, back_recv, (s, tp))

    for dt in range(1, T):
        gate_tp_copy(dt).start()

    def open_pairs(i, _):
        for dy in list(range(1, Y)) + [0]:
            pair_copy(source(i), dy).start()
        return 0

    lax.fori_loop(0, E, open_pairs, 0)

    def mix(s, dy):
        pair_copy(s, dy).wait_recv()
        return part[rows_of(s), cols_of(((y + dy) % Y) * 2 + c)].astype(F32) + pair_in[
            dy, rows_of(s), :
        ].astype(F32)

    def cross(s):
        for dy in range(1, Y):
            y_out[dy - 1, rows_of(s), :] = mix(s, dy).astype(BF16)
            y_copy(s, dy).start()

    def send_back(s):
        value = mix(s, 0)
        for dy in range(1, Y):
            y_copy(s, dy).wait_recv()
            value = value + y_in[dy - 1, rows_of(s), :].astype(F32)
        value = value.astype(BF16)

        @pl.when(s != me)
        def _():
            row_out[rows_of(s), :] = value
            back_copy(s).start()

        @pl.when(s == me)
        def _():
            back[me] = value

    def main(i, _):
        @pl.when(i < E)
        def _():
            cross(source(i))

        @pl.when(i >= 2)
        def _():
            send_back(source(i - 2))

        return 0

    lax.fori_loop(0, E + 2, main, 0)

    total = gate[...]
    for dt in range(1, T):
        gate_tp_copy(dt).wait()
        total = total + gate_in[dt]
    gate_out[...] = total
    gate_back[me] = gate_out[me]

    def gates(d, _):
        gate_ep_copy((me + d) % E).start()
        return 0

    lax.fori_loop(1, E, gates, 0)

    for dy in range(Y):
        everything = pair_in.at[dy]
        remote(everything, everything, pair_send.at[dy], pair_send.at[dy], (me, sib)).wait_send()
    for dy in range(1, Y):
        everything = y_in.at[dy - 1]
        remote(everything, everything, y_send.at[dy - 1], y_send.at[dy - 1], (me, sib)).wait_send()
    blocks = back.at[pl.ds(0, E - 1)]
    done = remote(blocks, blocks, back_send, back_recv, (me, sib))
    done.wait_send()
    done.wait_recv()
    blocks = gate_back.at[pl.ds(0, E - 1)]
    done = remote(blocks, blocks, gate_ep_send, gate_ep_recv, (me, sib))
    done.wait_send()
    done.wait_recv()


def expert_compute(
    dims, xfull, gfull, meta_out, hidden, grad_gate, grad_up, wg, wu, wd, accs, part, gate
):
    E, T, C, F, N = dims
    acc_g, acc_u, acc_b = accs.at[0], accs.at[1], accs.at[2]
    nt = (((1,), (1,)), ((), ()))
    accs[...] = jnp.zeros_like(accs)

    def forward(t, _):
        cols = pl.ds(pl.multiple_of(t * F, 128), F)
        acc_g[...] += lax.dot_general(
            xfull[:, cols], wg[:, cols], nt, preferred_element_type=F32
        )
        acc_u[...] += lax.dot_general(
            xfull[:, cols], wu[:, cols], nt, preferred_element_type=F32
        )
        acc_b[...] += lax.dot_general(
            gfull[:, cols], wd[:, cols], nt, preferred_element_type=F32
        )
        return 0

    lax.fori_loop(0, T, forward, 0)
    diagonal = lax.broadcasted_iota(jnp.int32, (C, 128), 0) == lax.broadcasted_iota(
        jnp.int32, (C, 128), 1
    )

    def middle(s, _):
        rows = pl.ds(pl.multiple_of(s * C, 16), C)
        pre_gate = acc_g[rows, :]
        pre_up = acc_u[rows, :]
        back = acc_b[rows, :]
        weight = meta_out[s, :, N : N + 128].astype(F32)
        weight = weight[:, 0:1] + weight[:, 1:2]
        sigmoid_gate = jax.nn.sigmoid(pre_gate)
        silu_gate = pre_gate * sigmoid_gate
        hid = (silu_gate * pre_up).astype(BF16)
        hidden[rows, :] = hid
        column = jnp.sum(hid.astype(F32) * back, axis=1, keepdims=True)
        line = jnp.sum(jnp.where(diagonal, column, 0.0), axis=0, keepdims=True)
        gate[s] = jnp.broadcast_to(line, (8, 128))
        scaled = weight * back
        grad_gate[rows, :] = (
            scaled * pre_up * sigmoid_gate * (1.0 + pre_gate * (1.0 - sigmoid_gate))
        ).astype(BF16)
        grad_up[rows, :] = (scaled * silu_gate).astype(BF16)
        return 0

    lax.fori_loop(0, E, middle, 0)

    def partial(t, _):
        cols = pl.ds(pl.multiple_of(t * F, 128), F)
        part[:, cols] = (
            jnp.dot(grad_gate[...], wg[:, cols], preferred_element_type=F32)
            + jnp.dot(grad_up[...], wu[:, cols], preferred_element_type=F32)
        ).astype(BF16)
        return 0

    lax.fori_loop(0, T, partial, 0)


def whole_kernel(dims, n_dispatch, *refs):
    E, T, X, C, F, N = dims
    tok, meta, cot, sh, w_gate, w_up, w_down = refs[:7]
    xfull, gfull, meta_out, cot_all, sh_out, hidden, grad_gate, grad_up, back, gate_back = refs[
        7:17
    ]
    wg, wu, wd, accs, part, gate, load_sem = refs[17:24]
    rest = refs[24:]
    loads = [
        pltpu.make_async_copy(src.at[0], dst, load_sem.at[i])
        for i, (src, dst) in enumerate(((w_gate, wg), (w_up, wu), (w_down, wd)))
    ]
    for cp in loads:
        cp.start()
    dispatch_kernel(
        dims,
        tok,
        meta,
        cot,
        sh,
        xfull,
        gfull,
        meta_out,
        cot_all,
        sh_out,
        *rest[:n_dispatch],
    )
    for cp in loads:
        cp.wait()
    expert_compute(
        (E, T, C, F, N),
        xfull,
        gfull,
        meta_out,
        hidden,
        grad_gate,
        grad_up,
        wg,
        wu,
        wd,
        accs,
        part,
        gate,
    )
    return_kernel((E, T, C, F), part, gate, back, gate_back, *rest[n_dispatch:])


def routed(E, T, C, F, N, rows, meta, cotangent, shared, w_gate, w_up, w_down):
    X = 2 if E % 2 == 0 else 1
    Y = T // 2
    Z = max(Y - 1, 1)
    R = E * C
    S = shared.shape[1]
    H = w_gate.shape[1]
    dma = pltpu.SemaphoreType.DMA
    vmem = pl.BlockSpec(memory_space=pltpu.VMEM)
    anywhere = pl.BlockSpec(memory_space=pl.ANY)
    shape = jax.ShapeDtypeStruct
    sems = [
        dma((4,)),
        dma((E,)),
        dma((E,)),
        dma((E,)),
        dma((E,)),
        dma((E,)),
        dma((E,)),
        dma((E,)),
        dma((E,)),
        dma((max(X - 1, 1), E)),
        dma((E,)),
        dma((2, Z)),
        dma((2, Z, E)),
        dma((2, Y)),
        dma((2, Y)),
    ]
    home = [
        pltpu.VMEM((Y, R, F), BF16),
        pltpu.VMEM((Z, R, F), BF16),
        pltpu.VMEM((Z, R, F), BF16),
        pltpu.VMEM((R, F), BF16),
        pltpu.VMEM((T, E, 8, 128), F32),
        pltpu.VMEM((E, 8, 128), F32),
        dma((Y,)),
        dma((Y, E)),
        dma((Z,)),
        dma((Z, E)),
        dma,
        dma,
        dma((T,)),
        dma((T,)),
        dma,
        dma,
    ]
    return pl.pallas_call(
        functools.partial(whole_kernel, (E, T, X, C, F, N), len(sems)),
        out_shape=(
            shape((R, T * F), BF16),
            shape((R, T * F), BF16),
            shape(meta.shape, BF16),
            shape((E, N, F), BF16),
            shape((S, E * N), BF16),
            shape((R, H), BF16),
            shape((R, H), BF16),
            shape((R, H), BF16),
            shape((E, C, F), BF16),
            shape((E, 8, 128), F32),
        ),
        in_specs=[vmem] * 4 + [anywhere] * 3,
        out_specs=(vmem,) * 10,
        scratch_shapes=[
            pltpu.VMEM((H, T * F), BF16),
            pltpu.VMEM((H, T * F), BF16),
            pltpu.VMEM((H, T * F), BF16),
            pltpu.VMEM((3, R, H), F32),
            pltpu.VMEM((R, T * F), BF16),
            pltpu.VMEM((E, 8, 128), F32),
            dma((3,)),
        ]
        + sems
        + home,
        compiler_params=pltpu.CompilerParams(
            collective_id=0, has_side_effects=True, vmem_limit_bytes=56 * 1024 * 1024
        ),
        name="routed",
    )(rows, meta, cotangent, shared, w_gate, w_up, w_down)


def shards(tokens, cotangent, routes, gate_weight, w_gate, w_up, w_down, shared_hidden):
    tok_count, top_count = routes.shape
    E = lax.axis_size("ep")
    T = lax.axis_size("tp")
    F = tokens.shape[1]
    capacity = 3 * tok_count * top_count // (2 * E)
    C = -(-capacity // 16) * 16
    R = E * C
    flat_routes = routes.reshape(-1)
    onehot = (flat_routes[:, None] == jnp.arange(E, dtype=jnp.int32)[None, :]).astype(F32)
    count = tok_count * top_count
    before = (
        jnp.arange(count, dtype=jnp.int32)[:, None] > jnp.arange(count, dtype=jnp.int32)[None, :]
    ).astype(BF16)
    earlier = jnp.dot(before, onehot.astype(BF16), preferred_element_type=F32)
    positions = jnp.sum(earlier * onehot, axis=1).astype(jnp.int32)
    slots = (flat_routes * C + positions).reshape(tok_count, top_count)
    lines = jnp.arange(R, dtype=jnp.int32)[:, None]
    masks = [slots[:, k][None, :] == lines for k in range(top_count)]
    select = functools.reduce(jnp.logical_or, masks).astype(BF16)
    weight = sum(
        jnp.sum(jnp.where(m, gate_weight[:, k][None, :], 0.0), axis=1)
        for k, m in enumerate(masks)
    )
    high = lax.reduce_precision(weight, 8, 7)
    low = weight - high
    tail = jnp.arange(128, dtype=jnp.int32)[None, :]
    extra = jnp.where(
        tail == 0, high[:, None], jnp.where(tail == 1, low[:, None], 0.0)
    ).astype(BF16)
    meta = jnp.concatenate([select, extra], axis=1).reshape(E, C, tok_count + 128)
    rows = jnp.dot(select, tokens, preferred_element_type=F32).astype(BF16).reshape(E, C, F)
    shared = shared_hidden.T.reshape(E, shared_hidden.shape[1] // E, tok_count)

    (
        rows_x,
        rows_g,
        meta_got,
        cot_all,
        shared_got,
        hidden,
        grad_pre_gate,
        grad_pre_up,
        back_rows,
        back_gate,
    ) = routed(
        E, T, C, F, tok_count, rows, meta, cotangent, shared, w_gate, w_up, w_down
    )
    got = meta_got.reshape(R, tok_count + 128)
    weight_col = got[:, tok_count : tok_count + 1].astype(F32) + got[
        :, tok_count + 1 : tok_count + 2
    ].astype(F32)
    weighted_cotan = (weight_col * rows_g.astype(F32)).astype(BF16)
    grad_down = jnp.dot(hidden.T, weighted_cotan, preferred_element_type=F32)
    grad_gate = jnp.dot(grad_pre_gate.T, rows_x, preferred_element_type=F32)
    grad_up = jnp.dot(grad_pre_up.T, rows_x, preferred_element_type=F32)
    shared_grad = jnp.dot(
        shared_got, cot_all.reshape(E * tok_count, F), preferred_element_type=F32
    )
    back_gate = back_gate[:, 0, :C]
    tokens_grad = lax.dot_general(
        select, back_rows.reshape(R, F), (((0,), (0,)), ((), ())), preferred_element_type=F32
    ).astype(BF16)
    gate_grad = jnp.stack(
        [jnp.sum(jnp.where(m, back_gate.reshape(R, 1), 0.0), axis=0) for m in masks], axis=1
    )
    return (tokens_grad, gate_grad, grad_gate[None], grad_up[None], grad_down[None], shared_grad)


def solution(mesh):
    placed = (
        P("ep", "tp"),
        P("ep", "tp"),
        P("ep", None),
        P("ep", None),
        P("ep", "tp", None),
        P("ep", "tp", None),
        P("ep", "tp", None),
        P("ep", None),
    )
    return jax.shard_map(
        shards,
        mesh=mesh,
        in_specs=placed,
        out_specs=(
            P("ep", "tp"),
            P("ep", None),
            P("ep", "tp", None),
            P("ep", "tp", None),
            P("ep", "tp", None),
            P("ep", "tp"),
        ),
        check_vma=False,
    )
```

profile of v0, /device:TPU:0, one launch (start us, length us, event | category | flops | bytes accessed | tf_op | source)
XLA Modules:
  0.0 131.0 jit_solution(4307778915708525839)
XLA Ops:
  0.6 0.8 slice_bitcast_fusion
  1.4 0.8 copy.33
  2.2 0.1 eq.91
  2.3 0.2 fusion.1
  2.6 0.1 convert_element_type.43
  2.8 0.7 multiply_add_fusion.1
  3.5 0.2 select_reduce_fusion.2
  3.8 0.2 select_convert_fusion
  3.9 0.1 or_convert_fusion
  4.1 0.7 pad_maximum_fusion.refs_1_
  4.8 1.8 %copy.35 = bf16[1024,128]{1,0:T(8,128)(2,1)} copy(bf16[1024,128]{0,1:T(8,128)(2,1)} %bitcast.35) | data formatting | bytes 524288 | tf_op jit(solution)/shard_map/transpose | solution.py:662
  6.6 1.2 convolution_convert_fusion
  7.8 102.5 %routed.1 = (bf16[384,4096]{1,0:T(8,128)(2,1)}, bf16[384,4096]{1,0:T(8,128)(2,1)}, bf16[8,48,256]{2,1,0:T(8,128)(2,1)}, bf16[8,128,1024]{2,1,0:T(8,128)(2,1)}, b...) custom-call(bf16[8,48,1024]{2,1,0:T(8,128)(2,1)} %bitcast.31, ...), custom_call_target="tpu_custom_call" | custom-call | tf_op jit(solution)/shard_map/routed/pallas_call | solution.py:596
  110.3 2.3 %convolution_convert_fusion.1 = bf16[128,1024]{1,0:T(8,128)(2,1)} fusion(bf16[384,1024]{1,0:T(8,128)(2,1)} %bitcast.34, s32[128]{0:T(128)S(1)} %get-tuple-element.35, s32[128]{0:T(128)S(1)} %get-tuple-element.34), kind=kOutput, calls=%fused_computation.6 | convolution fusion | flops 100941824 | bytes 1049600 | tf_op jit(solution)/shard_map/dot_general | solution.py:690
  112.6 0.8 slice_reduce_fusion
  113.5 0.1 select_reduce_fusion.1
  113.6 0.6 pad_maximum_fusion.1
  114.2 1.6 %fusion.10 = (bf16[384,1]{1,0:T(8,128)(2,1)}, bf16[384,1]{1,0:T(8,128)(2,1)S(1)}) fusion(bf16[384,256]{1,0:T(8,128)(2,1)} %bitcast.36), kind=kLoop, calls=%fused_computation.39 | loop fusion | bytes 3072 | tf_op jit(solution)/shard_map/slice | solution.py:679
  115.8 1.0 copy.38
  116.8 0.1 copy.39
  116.9 2.9 %fusion.12 = f32[128,1024]{1,0:T(8,128)} fusion(bf16[128,1024]{1,0:T(8,128)(2,1)} %get-tuple-element.24, bf16[1024,1024]{1,0:T(8,128)(2,1)} %bitcast.32), kind=kOutput, calls=%fused_computation.41 | convolution fusion | flops 268435456 | bytes 2883584 | tf_op jit(solution)/shard_map/dot_general | solution.py:686
  119.9 4.4 %convolution_bitcast_fusion = f32[1,256,4096]{2,1,0:T(8,128)} fusion(bf16[384,256]{1,0:T(8,128)(2,1)} %get-tuple-element.21, bf16[384,4096]{1,0:T(8,128)(2,1)S(1)} %copy-done.2, f32[384]{0:T(512)S(1)} %add_reduce_fusion), kind=kOutput, calls=%fused_computation.1 | convolution fusion | flops 810024960 | bytes 7538176 | tf_op jit(solution)/shard_map/dot_general | solution.py:683
  124.3 3.3 %convolution_bitcast_fusion.2 = f32[1,256,4096]{2,1,0:T(8,128)} fusion(bf16[384,256]{1,0:T(8,128)(2,1)S(1)} %copy-done.4, bf16[384,4096]{1,0:T(8,128)(2,1)S(1)} %copy-done.1), kind=kOutput, calls=%fused_computation.3 | convolution fusion | flops 805306368 | bytes 7536640 | tf_op jit(solution)/shard_map/dot_general | solution.py:684
  127.7 3.3 %convolution_bitcast_fusion.1 = f32[1,256,4096]{2,1,0:T(8,128)} fusion(bf16[384,256]{1,0:T(8,128)(2,1)S(1)} %copy-done.3, bf16[384,4096]{1,0:T(8,128)(2,1)S(1)} %copy-done.1), kind=kOutput, calls=%fused_computation.2 | convolution fusion | flops 805306368 | bytes 7536640 | tf_op jit(solution)/shard_map/dot_general | solution.py:685
  (20 shorter events, 0.3 us)
Async XLA Ops:
  0.6 5.9 %copy-start = (bf16[128,1024]{1,0:T(8,128)(2,1)S(1)}, bf16[128,1024]{1,0:T(8,128)(2,1)}, u32[]{:S(2)}) copy-start(bf16[128,1024]{1,0:T(8,128)(2,1)} %param.8) | copy-start | bytes 786436
  110.3 9.6 %copy-start.2 = (bf16[384,4096]{1,0:T(8,128)(2,1)S(1)}, bf16[384,4096]{1,0:T(8,128)(2,1)}, u32[]{:S(2)}) copy-start(bf16[384,4096]{1,0:T(8,128)(2,1)} %get-tuple-element.23) | copy-start | bytes 9437188
  119.9 4.5 %copy-start.1 = (bf16[384,4096]{1,0:T(8,128)(2,1)S(1)}, bf16[384,4096]{1,0:T(8,128)(2,1)}, u32[]{:S(2)}) copy-start(bf16[384,4096]{1,0:T(8,128)(2,1)} %get-tuple-element.19) | copy-start | bytes 9437188
  119.9 4.5 %copy-start.4 = (bf16[384,256]{1,0:T(8,128)(2,1)S(1)}, bf16[384,256]{1,0:T(8,128)(2,1)}, u32[]{:S(2)}) copy-start(bf16[384,256]{1,0:T(8,128)(2,1)} %get-tuple-element.18) | copy-start | bytes 589828
  124.3 3.3 %copy-start.3 = (bf16[384,256]{1,0:T(8,128)(2,1)S(1)}, bf16[384,256]{1,0:T(8,128)(2,1)}, u32[]{:S(2)}) copy-start(bf16[384,256]{1,0:T(8,128)(2,1)} %get-tuple-element.20) | copy-start | bytes 589828
where the time goes:
time: 131 us
  Pallas kernels  102 us (78%)
  matrix products  17.8 us (14%)
  local copies, waits for them, and re-layouts  7.33 us (6%)
  other arithmetic  2.67 us (2%)
    pallas_call x1, Pallas kernels, routed(): pl.pallas_call(functools.partial(whole_kernel, (E, T, X, C, F, N), len(se...  102 us
    dot_general x1, matrix products, shards(): grad_down = jnp.dot(hidden.T, weighted_cotan, preferred_element_type=F32)  4.45 us
    dot_general x1, matrix products, shards(): grad_up = jnp.dot(grad_pre_up.T, rows_x, preferred_element_type=F32)  3.3 us
    dot_general x1, matrix products, shards(): grad_gate = jnp.dot(grad_pre_gate.T, rows_x, preferred_element_type=F32)  3.3 us
    dot_general x1, matrix products, shards(): jnp.dot(shared_got, cot_all.reshape(E * tok_count, F), preferred_element_...  2.94 us

commit v1 on v0

v1 whole, which is shorter than its diff:
```python
import functools

import jax
import jax.numpy as jnp
from jax import lax
from jax.experimental import pallas as pl
from jax.experimental.pallas import tpu as pltpu
from jax.sharding import PartitionSpec as P

MESH = pl.DeviceIdType.MESH
BF16 = jnp.bfloat16
F32 = jnp.float32
NT = (((1,), (1,)), ((), ()))
TN = (((0,), (0,)), ((), ()))


def routed_kernel(dims, *refs):
    E, T, X, C, F, N, K, H, hs = dims
    Y = T // 2
    NZ = E // X
    G = X * C
    tok_hbm, cot_hbm, routes_hbm, gates_hbm, sh_hbm, w_gate, w_up, w_down = refs[:8]
    xfull, gfull, hidden, grad_gate, grad_up, tokens_grad, gate_grad, shared_grad = refs[8:16]
    (
        wg,
        wu,
        wd,
        rows_out,
        meta_out,
        meta_in,
        cot_all,
        sh_in,
        gx_out,
        accs,
        part,
        pair_in,
        y_out,
        y_in,
        row_out,
        back,
        gate,
        gate_in,
        gate_out,
        gate_back,
        table,
        tg_acc,
        sg_acc,
        sg_out,
        sg_in,
        sh_t,
        tok,
        cot,
        routes,
        gates,
        sh,
    ) = refs[16:47]
    (
        load_sem,
        local_sem,
        meta_send,
        meta_recv,
        tok_send,
        tok_recv,
        sh_send,
        sh_recv,
        cot_up,
        cot_down,
        cot_recv,
        gx_send,
        gx_recv,
        y_send,
        y_recv,
        sib_send,
        sib_recv,
        pair_send,
        pair_recv,
        yr_send,
        yr_recv,
        back_send,
        back_recv,
        gate_tp_send,
        gate_tp_recv,
        gate_ep_send,
        gate_ep_recv,
        sg_send,
        sg_recv,
    ) = refs[47:]
    full = (xfull, gfull)
    me = lax.axis_index("ep")
    tp = lax.axis_index("tp")
    y = tp // 2
    c = tp % 2
    sib = y * 2 + (1 - c)
    z = me // X
    x = me % X

    barrier = pltpu.get_barrier_semaphore()

    def greet(d, _):
        pl.semaphore_signal(
            barrier, inc=1, device_id=((me + d) % E, tp), device_id_type=MESH
        )
        return 0

    lax.fori_loop(1, E, greet, 0)
    for dt in range(1, T):
        pl.semaphore_signal(
            barrier, inc=1, device_id=(me, (tp + dt) % T), device_id_type=MESH
        )

    loads = [
        pltpu.make_async_copy(src.at[0], dst, load_sem.at[i])
        for i, (src, dst) in enumerate(((w_gate, wg), (w_up, wu), (w_down, wd)))
    ]
    fetches = [
        pltpu.make_async_copy(src, dst, local_sem.at[i])
        for i, (src, dst) in enumerate(
            (
                (routes_hbm, routes),
                (gates_hbm, gates),
                (tok_hbm, tok),
                (cot_hbm, cot),
                (cot_hbm, cot_all.at[z]),
                (sh_hbm, sh),
            )
        )
    ]
    for cp in fetches:
        cp.start()
    for cp in loads:
        cp.start()
    for cp in fetches[:2]:
        cp.wait()

    def rows_of(s):
        return pl.ds(pl.multiple_of(s * C, 16), C)

    def group_of(zs):
        return pl.ds(pl.multiple_of(zs * G, 16), G)

    def cols_of(t):
        return pl.ds(pl.multiple_of(t * F, 128), F)

    def hidden_plane(zd):
        return pl.ds(pl.multiple_of(zd * X * hs, 16), X * hs)

    def remote(src, dst, ss, rs, dev):
        return pltpu.make_async_remote_copy(
            src_ref=src,
            dst_ref=dst,
            send_sem=ss,
            recv_sem=rs,
            device_id=dev,
            device_id_type=MESH,
        )

    def plane(j):
        near = jnp.minimum(z, NZ - 1 - z)
        swing = z + ((j + 1) // 2) * (1 - 2 * (j % 2))
        far = jnp.where(z < NZ - 1 - z, j, NZ - 1 - j)
        return jnp.where(j <= 2 * near, swing, far)

    expert = lax.broadcasted_iota(jnp.int32, (E, N), 0)
    hits = [routes[k : k + 1, :] == expert for k in range(K)]
    chosen = functools.reduce(jnp.logical_or, hits)
    weights = sum(jnp.where(h, gates[k : k + 1, :], 0.0) for k, h in enumerate(hits))
    earlier = (
        lax.broadcasted_iota(jnp.int32, (N, N), 0) < lax.broadcasted_iota(jnp.int32, (N, N), 1)
    ).astype(BF16)
    position = jnp.dot(chosen.astype(BF16), earlier, preferred_element_type=F32)
    position = jnp.where(chosen, position, -1.0)
    for e in range(E):
        meta_out[e // X, e % X : e % X + 1, :] = position[e : e + 1, :]
        meta_out[e // X, X + e % X : X + e % X + 1, :] = weights[e : e + 1, :]
    meta_in[me] = meta_out[z]
    for cp in fetches[2:4]:
        cp.wait()
    slot = lax.broadcasted_iota(jnp.int32, (C, N), 0).astype(F32)

    def pick(ref, s, row):
        return slot == ref[s, pl.ds(row, 1), :]

    def select(i, _):
        e = (me + i) % E
        chosen_rows = pick(meta_out, e // X, e % X).astype(BF16)
        table[rows_of(e), :] = chosen_rows
        rows_out[e] = jnp.dot(chosen_rows, tok[...], preferred_element_type=F32).astype(BF16)
        return 0

    lax.fori_loop(0, E, select, 0)
    xfull[rows_of(me), cols_of(tp)] = rows_out[me]
    gfull[rows_of(me), cols_of(tp)] = jnp.dot(
        table[rows_of(me), :], cot[...], preferred_element_type=F32
    ).astype(BF16)
    for cp in fetches[4:]:
        cp.wait()
    sh_t[...] = sh[...].T
    sh_in[z] = sh_t[hidden_plane(z), :]
    with jax.named_scope("barrier"):
        pl.semaphore_wait(barrier, (E - 1) + (T - 1))

    def meta_copy(dst):
        return remote(
            meta_out.at[dst // X], meta_in.at[me], meta_send.at[dst], meta_recv.at[me], (dst, tp)
        )

    def meta_wait(s):
        remote(
            meta_out.at[0], meta_in.at[s], meta_send.at[s], meta_recv.at[s], (me, tp)
        ).wait_recv()

    def tok_copy(dst):
        return remote(
            rows_out.at[dst],
            xfull.at[rows_of(me), cols_of(tp)],
            tok_send.at[dst],
            tok_recv.at[me],
            (dst, tp),
        )

    def sh_copy(zd):
        return remote(
            sh_t.at[hidden_plane(zd)],
            sh_in.at[z],
            sh_send.at[zd],
            sh_recv.at[z],
            (zd * X + x, tp),
        )

    def cot_copy(zs, sems, dst):
        return remote(cot_all.at[zs], cot_all.at[zs], sems.at[zs], cot_recv.at[zs], (dst, tp))

    def spread_cot(zs, act):
        @pl.when((zs <= z) & (z + 1 < NZ))
        def _():
            act(cot_copy(zs, cot_up, me + X))

        @pl.when((zs >= z) & (z >= 1))
        def _():
            act(cot_copy(zs, cot_down, me - X))

    def start(cp):
        cp.start()

    def wait_send(cp):
        cp.wait_send()

    def gx_copy(zs, d):
        return remote(
            gx_out.at[zs, d - 1],
            gfull.at[rows_of(zs * X + x), cols_of(tp)],
            gx_send.at[zs, d - 1],
            gx_recv.at[zs * X + x],
            (z * X + (x + d) % X, tp),
        )

    def y_copy(a, s, dy):
        piece = full[a].at[rows_of(s), cols_of(tp)]
        return remote(
            piece,
            piece,
            y_send.at[a, dy - 1],
            y_recv.at[a, dy - 1, s],
            (me, ((y + dy) % Y) * 2 + c),
        )

    def sib_copy(a, s, dy):
        piece = full[a].at[rows_of(s), cols_of(((y + Y - dy) % Y) * 2 + c)]
        return remote(
            piece, piece, sib_send.at[a, dy], sib_recv.at[a, dy, s // X], (me, sib)
        )

    def forward(a, s):
        for dy in range(1, Y):
            y_copy(a, s, dy).start()
        sib_copy(a, s, 0).start()

    def cross(zs):
        s = zs * X + x
        for d in range(1, X):
            xd = (x + d) % X
            gx_out[zs, d - 1] = jnp.dot(
                pick(meta_in, s, xd).astype(BF16), cot_all[zs], preferred_element_type=F32
            ).astype(BF16)
            gx_copy(zs, d).start()

    def others(fn):
        def step(j, _):
            zs = plane(j)
            for d in range(X):
                s = zs * X + (x + d) % X

                @pl.when(s != me)
                def _():
                    fn(s)

            return 0

        lax.fori_loop(0, NZ, step, 0)

    spread_cot(z, start)
    others(lambda s: meta_copy(s).start())
    cross(z)
    forward(1, me)
    others(lambda s: tok_copy(s).start())
    forward(0, me)

    def send_sh(j, _):
        sh_copy(plane(j)).start()
        return 0

    lax.fori_loop(1, NZ, send_sh, 0)

    def receive(j):
        zs = plane(j)
        s = zs * X + x

        @pl.when(j > 0)
        def _():
            remote(
                cot_all.at[zs], cot_all.at[zs], cot_up.at[zs], cot_recv.at[zs], (me, tp)
            ).wait_recv()
            spread_cot(zs, start)
            meta_wait(s)
            cross(zs)
            gfull[rows_of(s), cols_of(tp)] = jnp.dot(
                pick(meta_in, s, x).astype(BF16), cot_all[zs], preferred_element_type=F32
            ).astype(BF16)
            forward(1, s)

        for d in range(X):
            s = zs * X + (x + d) % X

            @pl.when(s != me)
            def _():
                remote(
                    rows_out.at[0],
                    xfull.at[rows_of(s), cols_of(tp)],
                    tok_send.at[s],
                    tok_recv.at[s],
                    (me, tp),
                ).wait_recv()
                forward(0, s)

        for d in range(1, X):
            s = zs * X + (x + d) % X
            remote(
                gx_out.at[0, 0],
                gfull.at[rows_of(s), cols_of(tp)],
                gx_send.at[0, 0],
                gx_recv.at[s],
                (me, tp),
            ).wait_recv()
            forward(1, s)

    def relay(j):
        zs = plane(j)
        for d in range(X):
            s = zs * X + (x + d) % X
            for a in (0, 1):
                for dy in range(1, Y):
                    piece = full[a].at[rows_of(s), cols_of(((y + Y - dy) % Y) * 2 + c)]
                    remote(
                        piece, piece, y_send.at[a, dy - 1], y_recv.at[a, dy - 1, s], (me, tp)
                    ).wait_recv()
                    sib_copy(a, s, dy).start()
            if d > 0:
                meta_wait(s)
        for a in (0, 1):
            for dy in range(Y):
                piece = full[a].at[group_of(zs), cols_of(((y + Y - dy) % Y) * 2 + 1 - c)]
                remote(
                    piece, piece, sib_send.at[a, dy], sib_recv.at[a, dy, zs], (me, sib)
                ).wait_recv()

    def pair_copy(zs, dy):
        return remote(
            part.at[group_of(zs), cols_of(((y + dy) % Y) * 2 + 1 - c)],
            pair_in.at[dy, group_of(zs)],
            pair_send.at[dy],
            pair_recv.at[dy, zs],
            (me, sib),
        )

    def compute(j):
        zs = plane(j)
        rows = group_of(zs)
        accs[...] = jnp.zeros_like(accs)

        @pl.when(j == 0)
        def _():
            for cp in loads:
                cp.wait()

        def ahead(t, _):
            cols = cols_of(t)
            for i, (v, w) in enumerate(((xfull, wg), (xfull, wu), (gfull, wd))):
                accs[i] += lax.dot_general(
                    v[rows, cols], w[:, cols], NT, preferred_element_type=F32
                )
            return 0

        lax.fori_loop(0, T, ahead, 0)
        for d in range(X):
            s = zs * X + d
            mine = slice(d * C, (d + 1) * C)
            picked = pick(meta_in, s, x)
            weight = jnp.sum(
                jnp.where(picked, meta_in[s, pl.ds(X + x, 1), :], 0.0), axis=1, keepdims=True
            )
            pre_gate = accs[0, mine, :]
            pre_up = accs[1, mine, :]
            behind = accs[2, mine, :]
            sigmoid_gate = jax.nn.sigmoid(pre_gate)
            silu_gate = pre_gate * sigmoid_gate
            hid = (silu_gate * pre_up).astype(BF16).astype(F32)
            column = jnp.sum(hid * behind, axis=1, keepdims=True)
            gate[pl.ds(s, 1), :] = jnp.sum(
                jnp.where(picked, column, 0.0), axis=0, keepdims=True
            )
            scaled = weight * behind
            hidden[rows_of(s), :] = (weight * hid).astype(BF16)
            grad_gate[rows_of(s), :] = (
                scaled * pre_up * sigmoid_gate * (1.0 + pre_gate * (1.0 - sigmoid_gate))
            ).astype(BF16)
            grad_up[rows_of(s), :] = (scaled * silu_gate).astype(BF16)

        def partial(t, _):
            cols = cols_of(t)
            part[rows, cols] = (
                jnp.dot(grad_gate[rows, :], wg[:, cols], preferred_element_type=F32)
                + jnp.dot(grad_up[rows, :], wu[:, cols], preferred_element_type=F32)
            ).astype(BF16)
            return 0

        lax.fori_loop(0, T, partial, 0)
        for dy in list(range(1, Y)) + [0]:
            pair_copy(zs, dy).start()

    def gate_tp_copy(dt):
        return remote(
            gate, gate_in.at[dt], gate_tp_send.at[dt], gate_tp_recv.at[dt], (me, (tp + dt) % T)
        )

    def share(j):
        zs = plane(j)

        @pl.when(j > 0)
        def _():
            remote(
                sh_t.at[hidden_plane(0)], sh_in.at[zs], sh_send.at[zs], sh_recv.at[zs], (me, tp)
            ).wait_recv()

        sg_acc[...] += jnp.dot(sh_in[zs], cot_all[zs], preferred_element_type=F32)

    def mix(zs, dy):
        rows = group_of(zs)
        pair_copy(zs, dy).wait_recv()
        return part[rows, cols_of(((y + dy) % Y) * 2 + c)].astype(F32) + pair_in[
            dy, rows, :
        ].astype(F32)

    def return_y(zs, dy):
        rows = group_of(zs)
        return remote(
            y_out.at[dy - 1, rows],
            y_in.at[dy - 1, rows],
            yr_send.at[dy - 1],
            yr_recv.at[dy - 1, zs],
            (me, ((y + dy) % Y) * 2 + c),
        )

    def combine(j):
        zs = plane(j)
        for dy in range(1, Y):
            y_out[dy - 1, group_of(zs), :] = mix(zs, dy).astype(BF16)
            return_y(zs, dy).start()

    def back_copy(s):
        return remote(
            row_out.at[rows_of(s)], back.at[rows_of(me)], back_send, back_recv.at[me], (s, tp)
        )

    def send_back(j):
        zs = plane(j)
        value = mix(zs, 0)
        for dy in range(1, Y):
            return_y(zs, dy).wait_recv()
            value = value + y_in[dy - 1, group_of(zs), :].astype(F32)
        row_out[group_of(zs), :] = value.astype(BF16)
        for d in range(X):
            s = zs * X + d

            @pl.when(s != me)
            def _():
                back_copy(s).start()

            @pl.when(s == me)
            def _():
                back[rows_of(s), :] = row_out[rows_of(s), :]

    sg_acc[...] = jnp.zeros_like(sg_acc)

    def main(i, _):
        @pl.when(i < NZ)
        def _():
            with jax.named_scope("receive"):
                receive(i)

        @pl.when((i >= 1) & (i <= NZ))
        def _():
            with jax.named_scope("relay"):
                relay(i - 1)
            with jax.named_scope("compute"):
                compute(i - 1)

        @pl.when(i == NZ)
        def _():
            for dt in range(1, T):
                gate_tp_copy(dt).start()

        @pl.when((i >= 1) & (i <= NZ))
        def _():
            with jax.named_scope("share"):
                share(i - 1)
            with jax.named_scope("combine"):
                combine(i - 1)

        @pl.when(i >= 2)
        def _():
            with jax.named_scope("send_back"):
                send_back(i - 2)

        return 0

    lax.fori_loop(0, NZ + 2, main, 0)

    def sg_copy(d):
        return remote(
            sg_out.at[d - 1],
            sg_in.at[d - 1],
            sg_send.at[d - 1],
            sg_recv.at[d - 1],
            (z * X + (x + d) % X, tp),
        )

    def hidden_of(xd):
        return pl.ds(pl.multiple_of(xd * hs, 16), hs)

    for d in range(1, X):
        sg_out[d - 1] = sg_acc[hidden_of((x + d) % X), :].astype(BF16)
        sg_copy(d).start()

    total = gate[...]
    for dt in range(1, T):
        gate_tp_copy(dt).wait()
        total = total + gate_in[dt]
    gate_out[...] = total
    gate_back[me] = total

    def gate_ep_copy(s):
        return remote(gate_out, gate_back.at[me], gate_ep_send, gate_ep_recv.at[me], (s, tp))

    others(lambda s: gate_ep_copy(s).start())

    value = sg_acc[hidden_of(x), :]
    for d in range(1, X):
        sg_copy(d).wait()
        value = value + sg_in[d - 1].astype(F32)
    shared_grad[...] = value

    tg_acc[...] = jnp.zeros_like(tg_acc)

    def gather(j, _):
        zs = plane(j)
        for d in range(X):
            e = zs * X + d

            @pl.when(e != me)
            def _():
                remote(
                    row_out.at[rows_of(e)],
                    back.at[rows_of(e)],
                    back_send,
                    back_recv.at[e],
                    (me, tp),
                ).wait_recv()

        tg_acc[...] += lax.dot_general(
            table[group_of(zs), :], back[group_of(zs), :], TN, preferred_element_type=F32
        )
        return 0

    with jax.named_scope("gather"):
        lax.fori_loop(0, NZ, gather, 0)
    tokens_grad[...] = tg_acc[...].astype(BF16)

    def take_gates(e, values):
        @pl.when(e != me)
        def _():
            remote(
                gate_out, gate_back.at[e], gate_ep_send, gate_ep_recv.at[e], (me, tp)
            ).wait_recv()

        row = gate_back[e, pl.ds(me, 1), :]
        return values + jnp.where(routes[...] == e, row, 0.0)

    gate_grad[...] = lax.fori_loop(0, E, take_gates, jnp.zeros((K, N), F32))

    def finish(s):
        meta_copy(s).wait_send()
        tok_copy(s).wait_send()
        gate_ep_copy(s).wait_send()
        back_copy(s).wait_send()

    others(finish)

    def finish_plane(j, _):
        zs = plane(j)

        @pl.when(j > 0)
        def _():
            sh_copy(zs).wait_send()

        spread_cot(zs, wait_send)
        for d in range(1, X):
            gx_copy(zs, d).wait_send()
        return 0

    lax.fori_loop(0, NZ, finish_plane, 0)
    for a in (0, 1):
        piece = full[a].at[:, cols_of(tp)]
        for dy in range(1, Y):
            remote(
                piece, piece, y_send.at[a, dy - 1], y_send.at[a, dy - 1], (me, sib)
            ).wait_send()
        for dy in range(Y):
            remote(
                piece, piece, sib_send.at[a, dy], sib_send.at[a, dy], (me, sib)
            ).wait_send()
    for dy in range(Y):
        piece = pair_in.at[dy]
        remote(piece, piece, pair_send.at[dy], pair_send.at[dy], (me, sib)).wait_send()
    for dy in range(1, Y):
        piece = y_in.at[dy - 1]
        remote(piece, piece, yr_send.at[dy - 1], yr_send.at[dy - 1], (me, sib)).wait_send()


def routed(E, T, C, F, N, hs, tokens, cotangent, routes, gates, shared, w_gate, w_up, w_down):
    X = 2 if E % 2 == 0 else 1
    NZ = E // X
    Y = T // 2
    Z = max(Y - 1, 1)
    XO = max(X - 1, 1)
    R = E * C
    H = w_gate.shape[1]
    K = routes.shape[0]
    M = -(-2 * X // 8) * 8
    dma = pltpu.SemaphoreType.DMA
    vmem = pl.BlockSpec(memory_space=pltpu.VMEM)
    hbm = pl.BlockSpec(memory_space=pltpu.HBM)
    shape = jax.ShapeDtypeStruct
    buffers = [
        pltpu.VMEM((H, T * F), BF16),
        pltpu.VMEM((H, T * F), BF16),
        pltpu.VMEM((H, T * F), BF16),
        pltpu.VMEM((E, C, F), BF16),
        pltpu.VMEM((NZ, M, N), F32),
        pltpu.VMEM((E, M, N), F32),
        pltpu.VMEM((NZ, N, F), BF16),
        pltpu.VMEM((NZ, X * hs, N), BF16),
        pltpu.VMEM((NZ, XO, C, F), BF16),
        pltpu.VMEM((3, X * C, H), F32),
        pltpu.VMEM((R, T * F), BF16),
        pltpu.VMEM((Y, R, F), BF16),
        pltpu.VMEM((Z, R, F), BF16),
        pltpu.VMEM((Z, R, F), BF16),
        pltpu.VMEM((R, F), BF16),
        pltpu.VMEM((R, F), BF16),
        pltpu.VMEM((E, N), F32),
        pltpu.VMEM((T, E, N), F32),
        pltpu.VMEM((E, N), F32),
        pltpu.VMEM((E, E, N), F32),
        pltpu.VMEM((R, N), BF16),
        pltpu.VMEM((N, F), F32),
        pltpu.VMEM((X * hs, F), F32),
        pltpu.VMEM((XO, hs, F), BF16),
        pltpu.VMEM((XO, hs, F), BF16),
        pltpu.VMEM((E * hs, N), BF16),
        pltpu.VMEM((N, F), BF16),
        pltpu.VMEM((N, F), BF16),
        pltpu.VMEM((K, N), jnp.int32),
        pltpu.VMEM((K, N), F32),
        pltpu.VMEM((N, E * hs), BF16),
    ]
    sems = [
        dma((3,)),
        dma((6,)),
        dma((E,)),
        dma((E,)),
        dma((E,)),
        dma((E,)),
        dma((NZ,)),
        dma((NZ,)),
        dma((NZ,)),
        dma((NZ,)),
        dma((NZ,)),
        dma((NZ, XO)),
        dma((E,)),
        dma((2, Z)),
        dma((2, Z, E)),
        dma((2, Y)),
        dma((2, Y, NZ)),
        dma((Y,)),
        dma((Y, NZ)),
        dma((Z,)),
        dma((Z, NZ)),
        dma,
        dma((E,)),
        dma((T,)),
        dma((T,)),
        dma,
        dma((E,)),
        dma((XO,)),
        dma((XO,)),
    ]
    return pl.pallas_call(
        functools.partial(routed_kernel, (E, T, X, C, F, N, K, H, hs)),
        out_shape=(
            shape((R, T * F), BF16),
            shape((R, T * F), BF16),
            shape((R, H), BF16),
            shape((R, H), BF16),
            shape((R, H), BF16),
            shape((N, F), BF16),
            shape((K, N), F32),
            shape((hs, F), F32),
        ),
        in_specs=[hbm] * 8,
        out_specs=(vmem,) * 8,
        scratch_shapes=buffers + sems,
        compiler_params=pltpu.CompilerParams(
            collective_id=0, has_side_effects=True, vmem_limit_bytes=36 * 1024 * 1024
        ),
        name="routed",
    )(
        *(
            pltpu.with_memory_space_constraint(v, pltpu.HBM)
            for v in (tokens, cotangent, routes, gates, shared, w_gate, w_up, w_down)
        )
    )


def weights_kernel(
    tile,
    rows_x,
    rows_g,
    hidden,
    grad_gate,
    grad_up,
    tokens_in,
    shared_in,
    gate_in,
    out_gate,
    out_up,
    out_down,
    tokens_out,
    shared_out,
    gate_out,
    buf,
    sem,
    small_sem,
):
    small = (
        pltpu.make_async_copy(tokens_in, tokens_out, small_sem.at[0]),
        pltpu.make_async_copy(shared_in, shared_out, small_sem.at[1]),
        pltpu.make_async_copy(gate_in, gate_out, small_sem.at[2]),
    )
    for cp in small:
        cp.start()
    plan = ((grad_gate, rows_x, out_gate), (grad_up, rows_x, out_up), (hidden, rows_g, out_down))
    steps = rows_x.shape[1] // tile

    def drain(i, slot, w):
        cols = pl.ds(pl.multiple_of(i * tile, 128), tile)
        return pltpu.make_async_copy(
            buf.at[slot, w], plan[w][2].at[0, :, cols], sem.at[slot, w]
        )

    def step(i, _):
        slot = i % 2
        cols = pl.ds(pl.multiple_of(i * tile, 128), tile)
        for w, (left, right, _) in enumerate(plan):

            @pl.when(i >= 2)
            def _():
                drain(i - 2, slot, w).wait()

            buf[slot, w] = lax.dot_general(
                left[...], right[:, cols], TN, preferred_element_type=F32
            )
            drain(i, slot, w).start()
        return 0

    lax.fori_loop(0, steps, step, 0)
    for i in range(max(steps - 2, 0), steps):
        for w in range(3):
            drain(i, i % 2, w).wait()
    for cp in small:
        cp.wait()


def weight_grads(
    rows_x, rows_g, hidden, grad_gate, grad_up, tokens_grad, shared_grad, gate_grad
):
    H = hidden.shape[1]
    D = rows_x.shape[1]
    tile = 512 if D % 512 == 0 else 128
    vmem = pl.BlockSpec(memory_space=pltpu.VMEM)
    hbm = pl.BlockSpec(memory_space=pltpu.HBM)
    shape = jax.ShapeDtypeStruct
    return pl.pallas_call(
        functools.partial(weights_kernel, tile),
        out_shape=(
            shape((1, H, D), F32),
            shape((1, H, D), F32),
            shape((1, H, D), F32),
            shape(tokens_grad.shape, BF16),
            shape(shared_grad.shape, F32),
            shape(gate_grad.shape, F32),
        ),
        in_specs=[vmem] * 8,
        out_specs=(hbm,) * 6,
        scratch_shapes=[
            pltpu.VMEM((2, 3, H, tile), F32),
            pltpu.SemaphoreType.DMA((2, 3)),
            pltpu.SemaphoreType.DMA((3,)),
        ],
        compiler_params=pltpu.CompilerParams(vmem_limit_bytes=16 * 1024 * 1024),
        name="weight_grads",
    )(rows_x, rows_g, hidden, grad_gate, grad_up, tokens_grad, shared_grad, gate_grad)


def shards(tokens, cotangent, routes, gate_weight, w_gate, w_up, w_down, shared_hidden):
    tok_count, top_count = routes.shape
    E = lax.axis_size("ep")
    T = lax.axis_size("tp")
    F = tokens.shape[1]
    capacity = 3 * tok_count * top_count // (2 * E)
    C = -(-capacity // 16) * 16
    hs = shared_hidden.shape[1] // E
    rows_x, rows_g, hidden, grad_gate, grad_up, tokens_grad, gate_grad, shared_grad = routed(
        E,
        T,
        C,
        F,
        tok_count,
        hs,
        tokens,
        cotangent,
        routes.T,
        gate_weight.T,
        shared_hidden,
        w_gate,
        w_up,
        w_down,
    )
    out_gate, out_up, out_down, tokens_grad, shared_grad, gate_grad = weight_grads(
        rows_x, rows_g, hidden, grad_gate, grad_up, tokens_grad, shared_grad, gate_grad
    )
    return (tokens_grad, gate_grad.T, out_gate, out_up, out_down, shared_grad)


def solution(mesh):
    placed = (
        P("ep", "tp"),
        P("ep", "tp"),
        P("ep", None),
        P("ep", None),
        P("ep", "tp", None),
        P("ep", "tp", None),
        P("ep", "tp", None),
        P("ep", None),
    )
    return jax.shard_map(
        shards,
        mesh=mesh,
        in_specs=placed,
        out_specs=(
            P("ep", "tp"),
            P("ep", None),
            P("ep", "tp", None),
            P("ep", "tp", None),
            P("ep", "tp", None),
            P("ep", "tp"),
        ),
        check_vma=False,
    )
```

time: 131 us -> 98.7 us (0.75)
  matrix products: 17.8 us -> 0 us
  local copies, waits for them, and re-layouts: 7.33 us -> 0 us
  Pallas kernels: 102 us -> 97.9 us
  other arithmetic: 2.67 us -> 0 us
    dot_general x7 -> x0, matrix products: 17.8 us -> none  [the longest x1 4.45 us: shards(): grad_down = jnp.dot(hidden.T, weighted_cotan, preferred_element_type=F32)]
    pallas_call x1 -> x2, Pallas kernels: 102 us -> 97.9 us  [the longest x1 89.2 us: routed(): pl.pallas_call(functools.partial(routed_kernel, (E, T, X, C, F, N, K, H,...]
    slice x2 -> x0, local copies, waits for them, and re-layouts: 2.4 us -> none  [the longest x1 1.63 us: shards(): got[:, tok_count:tok_count + 1].astype(F32)]
    unnamed x13 -> x0, local copies, waits for them, and re-layouts: 1.89 us -> none
    transpose x1 -> x0, local copies, waits for them, and re-layouts: 1.79 us -> none  [shards(): shared = shared_hidden.T.reshape(E, shared_hidden.shape[1] // E, tok_count)]
where the time goes in v1:
time: 98.7 us; the launch traced here: 98.5 us
  Pallas kernels  97.9 us (99%)
    pallas_call x1, Pallas kernels, routed(): pl.pallas_call(functools.partial(routed_kernel, (E, T, X, C, F, N, K, H,...  89.2 us
    pallas_call x1, Pallas kernels, weight_grads(): pl.pallas_call(functools.partial(weights_kernel, tile), out_shape=(shape(...  8.69 us

profile of v1, /device:TPU:0, one launch (start us, length us, event | category | flops | bytes accessed | tf_op | source)
XLA Modules:
  0.0 98.5 jit_solution(15420652867941003074)
XLA Ops:
  0.6 89.2 %routed.1 = (bf16[384,4096]{1,0:T(8,128)(2,1)S(1)}, bf16[384,4096]{1,0:T(8,128)(2,1)S(1)}, bf16[384,256]{1,0:T(8,128)(2,1)S(1)}, bf16[384,256]{1,0:T(8,128)(2,1)...) custom-call(bf16[128,1024]{1,0:T(8,128)(2,1)} %refs_0_.1, ...), custom_call_target="tpu_custom_call" | custom-call | tf_op jit(solution)/shard_map/routed/pallas_call | solution.py:727
  89.8 8.7 %weight_grads.1 = (f32[1,256,4096]{2,1,0:T(8,128)}, f32[1,256,4096]{2,1,0:T(8,128)}, f32[1,256,4096]{2,1,0:T(8,128)}, bf16[128,1024]{1,0:T(8,128)(2,1)}, f32[128,1024]{1,0:T(8,128)}, /*index=5*/f32[2,128]{1,0:T(2,128)}) custom-call(bf16[384,4096]{1,0:T(8,128)(2,1)S(1)} %get-tuple-element.20.rows_x, bf16[384,4096]{1,0:T(8,128)(2,1)S(1)} %get-tuple-element.21.rows_g, ...), custom_call_target="tpu_custom_call" | custom-call | tf_op jit(solution)/shard_map/weight_grads/pallas_call | solution.py:822

commit v2 on v1

--- a/solution.py
+++ b/solution.py
@@ -20,7 +20,7 @@
     NZ = E // X
     G = X * C
     tok_hbm, cot_hbm, routes_hbm, gates_hbm, sh_hbm, w_gate, w_up, w_down = refs[:8]
-    xfull, gfull, hidden, grad_gate, grad_up, tokens_grad, gate_grad, shared_grad = refs[8:16]
+    out_gate, out_up, out_down, tokens_grad, gate_grad, shared_grad = refs[8:14]
     (
         wg,
         wu,
@@ -53,7 +53,14 @@
         routes,
         gates,
         sh,
-    ) = refs[16:47]
+        hid,
+        gg,
+        gu,
+        turned,
+        xfull,
+        gfull,
+        sides,
+    ) = refs[14:52]
     (
         load_sem,
         local_sem,
@@ -84,7 +91,9 @@
         gate_ep_recv,
         sg_send,
         sg_recv,
-    ) = refs[47:]
+        half_send,
+        half_recv,
+    ) = refs[52:]
     full = (xfull, gfull)
     me = lax.axis_index("ep")
     tp = lax.axis_index("tp")
@@ -127,8 +136,6 @@
     ]
     for cp in fetches:
         cp.start()
-    for cp in loads:
-        cp.start()
     for cp in fetches[:2]:
         cp.wait()
 
@@ -143,6 +150,11 @@
 
     def hidden_plane(zd):
         return pl.ds(pl.multiple_of(zd * X * hs, 16), X * hs)
+
+    half = X * hs // 2
+
+    def half_of(core):
+        return pl.ds(pl.multiple_of(core * half, 16), half)
 
     def remote(src, dst, ss, rs, dev):
         return pltpu.make_async_remote_copy(
@@ -154,8 +166,9 @@
             device_id_type=MESH,
         )
 
+    near = jnp.minimum(z, NZ - 1 - z)
+
     def plane(j):
-        near = jnp.minimum(z, NZ - 1 - z)
         swing = z + ((j + 1) // 2) * (1 - 2 * (j % 2))
         far = jnp.where(z < NZ - 1 - z, j, NZ - 1 - j)
         return jnp.where(j <= 2 * near, swing, far)
@@ -180,22 +193,16 @@
     def pick(ref, s, row):
         return slot == ref[s, pl.ds(row, 1), :]
 
-    def select(i, _):
-        e = (me + i) % E
+    def select(e):
         chosen_rows = pick(meta_out, e // X, e % X).astype(BF16)
         table[rows_of(e), :] = chosen_rows
         rows_out[e] = jnp.dot(chosen_rows, tok[...], preferred_element_type=F32).astype(BF16)
-        return 0
-
-    lax.fori_loop(0, E, select, 0)
-    xfull[rows_of(me), cols_of(tp)] = rows_out[me]
+
     gfull[rows_of(me), cols_of(tp)] = jnp.dot(
-        table[rows_of(me), :], cot[...], preferred_element_type=F32
+        pick(meta_out, z, x).astype(BF16), cot[...], preferred_element_type=F32
     ).astype(BF16)
     for cp in fetches[4:]:
         cp.wait()
-    sh_t[...] = sh[...].T
-    sh_in[z] = sh_t[hidden_plane(z), :]
     with jax.named_scope("barrier"):
         pl.semaphore_wait(barrier, (E - 1) + (T - 1))
 
@@ -220,8 +227,8 @@
 
     def sh_copy(zd):
         return remote(
-            sh_t.at[hidden_plane(zd)],
-            sh_in.at[z],
+            sh_t.at[pl.ds(pl.multiple_of(zd * X * hs + c * half, 16), half)],
+            sh_in.at[z, half_of(c)],
             sh_send.at[zd],
             sh_recv.at[z],
             (zd * X + x, tp),
@@ -299,35 +306,63 @@
         lax.fori_loop(0, NZ, step, 0)
 
     spread_cot(z, start)
+    forward(1, me)
     others(lambda s: meta_copy(s).start())
+    for cp in loads:
+        cp.start()
+
+    def send_rows(j):
+        zs = plane(j)
+        for d in range(X):
+            s = zs * X + (x + d) % X
+            select(s)
+
+            @pl.when(s != me)
+            def _():
+                tok_copy(s).start()
+
+    for d in range(1, X):
+        select(z * X + (x + d) % X)
+        tok_copy(z * X + (x + d) % X).start()
+    send_rows(1)
+    select(me)
+    xfull[rows_of(me), cols_of(tp)] = rows_out[me]
+    forward(0, me)
     cross(z)
-    forward(1, me)
-    others(lambda s: tok_copy(s).start())
-    forward(0, me)
-
-    def send_sh(j, _):
-        sh_copy(plane(j)).start()
-        return 0
-
-    lax.fori_loop(1, NZ, send_sh, 0)
-
-    def receive(j):
+
+    @pl.when(near >= 1)
+    def _():
+        send_rows(2)
+
+    def send_late(i):
+        j = jnp.where(near >= 1, i + 2, i + 1)
+
+        @pl.when(j < NZ)
+        def _():
+            send_rows(j)
+
+    sh_t[...] = sh[...].T
+    sh_in[z] = sh_t[hidden_plane(z), :]
+
+    def take_block(j):
+        zs = plane(j)
+        remote(
+            cot_all.at[zs], cot_all.at[zs], cot_up.at[zs], cot_recv.at[zs], (me, tp)
+        ).wait_recv()
+        spread_cot(zs, start)
+
+    def use_block(j):
         zs = plane(j)
         s = zs * X + x
-
-        @pl.when(j > 0)
-        def _():
-            remote(
-                cot_all.at[zs], cot_all.at[zs], cot_up.at[zs], cot_recv.at[zs], (me, tp)
-            ).wait_recv()
-            spread_cot(zs, start)
-            meta_wait(s)
-            cross(zs)
-            gfull[rows_of(s), cols_of(tp)] = jnp.dot(
-                pick(meta_in, s, x).astype(BF16), cot_all[zs], preferred_element_type=F32
-            ).astype(BF16)
-            forward(1, s)
-
+        meta_wait(s)
+        cross(zs)
+        gfull[rows_of(s), cols_of(tp)] = jnp.dot(
+            pick(meta_in, s, x).astype(BF16), cot_all[zs], preferred_element_type=F32
+        ).astype(BF16)
+        forward(1, s)
+
+    def tokens_in(j):
+        zs = plane(j)
         for d in range(X):
             s = zs * X + (x + d) % X
 
@@ -342,6 +377,8 @@
                 ).wait_recv()
                 forward(0, s)
 
+    def crossed(j):
+        zs = plane(j)
         for d in range(1, X):
             s = zs * X + (x + d) % X
             remote(
@@ -352,6 +389,27 @@
                 (me, tp),
             ).wait_recv()
             forward(1, s)
+
+    def arrivals(i):
+        first = (near == 0) | (i == 1)
+        second = (near >= 1) & (i + 1 < NZ)
+        for fn in (take_block, use_block, None, tokens_in, crossed):
+            if fn is None:
+                send_late(i)
+                continue
+            with jax.named_scope(fn.__name__):
+
+                @pl.when(first)
+                def _():
+                    fn(i)
+
+                @pl.when(second)
+                def _():
+                    fn(i + 1)
+
+    def send_shared(j, _):
+        sh_copy(plane(j)).start()
+        return 0
 
     def relay(j):
         zs = plane(j)
@@ -385,22 +443,9 @@
     def compute(j):
         zs = plane(j)
         rows = group_of(zs)
-        accs[...] = jnp.zeros_like(accs)
-
-        @pl.when(j == 0)
-        def _():
-            for cp in loads:
-                cp.wait()
-
-        def ahead(t, _):
-            cols = cols_of(t)
-            for i, (v, w) in enumerate(((xfull, wg), (xfull, wu), (gfull, wd))):
-                accs[i] += lax.dot_general(
-                    v[rows, cols], w[:, cols], NT, preferred_element_type=F32
-                )
-            return 0
-
-        lax.fori_loop(0, T, ahead, 0)
+        with jax.named_scope("ahead"):
+            for i, v in enumerate((xfull, xfull, gfull)):
+                accs[i] = jnp.dot(v[rows, :], turned[i], preferred_element_type=F32)
         for d in range(X):
             s = zs * X + d
             mine = slice(d * C, (d + 1) * C)
@@ -413,45 +458,61 @@
             behind = accs[2, mine, :]
             sigmoid_gate = jax.nn.sigmoid(pre_gate)
             silu_gate = pre_gate * sigmoid_gate
-            hid = (silu_gate * pre_up).astype(BF16).astype(F32)
-            column = jnp.sum(hid * behind, axis=1, keepdims=True)
+            act = (silu_gate * pre_up).astype(BF16).astype(F32)
+            column = jnp.sum(act * behind, axis=1, keepdims=True)
             gate[pl.ds(s, 1), :] = jnp.sum(
                 jnp.where(picked, column, 0.0), axis=0, keepdims=True
             )
             scaled = weight * behind
-            hidden[rows_of(s), :] = (weight * hid).astype(BF16)
-            grad_gate[rows_of(s), :] = (
+            hid[rows_of(s), :] = (weight * act).astype(BF16)
+            gg[rows_of(s), :] = (
                 scaled * pre_up * sigmoid_gate * (1.0 + pre_gate * (1.0 - sigmoid_gate))
             ).astype(BF16)
-            grad_up[rows_of(s), :] = (scaled * silu_gate).astype(BF16)
-
-        def partial(t, _):
-            cols = cols_of(t)
+            gu[rows_of(s), :] = (scaled * silu_gate).astype(BF16)
+
+    def spread_rows(j):
+        zs = plane(j)
+        rows = group_of(zs)
+
+        def partial(i, _):
+            cols = cols_of((i % Y) * 2 + jnp.where(i < Y, 1 - c, c))
             part[rows, cols] = (
-                jnp.dot(grad_gate[rows, :], wg[:, cols], preferred_element_type=F32)
-                + jnp.dot(grad_up[rows, :], wu[:, cols], preferred_element_type=F32)
+                jnp.dot(gg[rows, :], wg[:, cols], preferred_element_type=F32)
+                + jnp.dot(gu[rows, :], wu[:, cols], preferred_element_type=F32)
             ).astype(BF16)
             return 0
 
-        lax.fori_loop(0, T, partial, 0)
+        with jax.named_scope("partial"):
+            lax.fori_loop(0, Y, partial, 0)
         for dy in list(range(1, Y)) + [0]:
             pair_copy(zs, dy).start()
+        lax.fori_loop(Y, T, partial, 0)
 
     def gate_tp_copy(dt):
         return remote(
             gate, gate_in.at[dt], gate_tp_send.at[dt], gate_tp_recv.at[dt], (me, (tp + dt) % T)
         )
 
-    def share(j):
+    def half_copy(zs, core):
+        piece = sh_in.at[zs, half_of(core)]
+        return remote(piece, piece, half_send.at[zs], half_recv.at[zs], (me, sib))
+
+    def half_relay(j, _):
+        zs = plane(j)
+        piece = sh_in.at[zs, half_of(c)]
+        remote(piece, piece, sh_send.at[zs], sh_recv.at[zs], (me, tp)).wait_recv()
+        half_copy(zs, c).start()
+        return 0
+
+    def share(j, _):
         zs = plane(j)
 
         @pl.when(j > 0)
         def _():
-            remote(
-                sh_t.at[hidden_plane(0)], sh_in.at[zs], sh_send.at[zs], sh_recv.at[zs], (me, tp)
-            ).wait_recv()
+            half_copy(zs, 1 - c).wait_recv()
 
         sg_acc[...] += jnp.dot(sh_in[zs], cot_all[zs], preferred_element_type=F32)
+        return 0
 
     def mix(zs, dy):
         rows = group_of(zs)
@@ -501,40 +562,6 @@
 
     sg_acc[...] = jnp.zeros_like(sg_acc)
 
-    def main(i, _):
-        @pl.when(i < NZ)
-        def _():
-            with jax.named_scope("receive"):
-                receive(i)
-
-        @pl.when((i >= 1) & (i <= NZ))
-        def _():
-            with jax.named_scope("relay"):
-                relay(i - 1)
-            with jax.named_scope("compute"):
-                compute(i - 1)
-
-        @pl.when(i == NZ)
-        def _():
-            for dt in range(1, T):
-                gate_tp_copy(dt).start()
-
-        @pl.when((i >= 1) & (i <= NZ))
-        def _():
-            with jax.named_scope("share"):
-                share(i - 1)
-            with jax.named_scope("combine"):
-                combine(i - 1)
-
-        @pl.when(i >= 2)
-        def _():
-            with jax.named_scope("send_back"):
-                send_back(i - 2)
-
-        return 0
-
-    lax.fori_loop(0, NZ + 2, main, 0)
-
     def sg_copy(d):
         return remote(
             sg_out.at[d - 1],
@@ -547,13 +574,109 @@
     def hidden_of(xd):
         return pl.ds(pl.multiple_of(xd * hs, 16), hs)
 
-    for d in range(1, X):
-        sg_out[d - 1] = sg_acc[hidden_of((x + d) % X), :].astype(BF16)
-        sg_copy(d).start()
+    def turn(k):
+        inward = jnp.where(2 * z < NZ - 1, 2, 1)
+        outward = 3 - inward
+        middle = jnp.where(k == 0, inward, jnp.where(k == 1, outward, (k + 1) % NZ))
+        return jnp.where(near >= 1, middle, k)
+
+    D = T * F
+    tile = 512 if D % 512 == 0 else 128
+
+    def weights_up():
+        for n, src in enumerate((gg, gu, hid)):
+            sides[n * H : (n + 1) * H, :] = src[...].T
+
+        def step(i, _):
+            cols = pl.ds(pl.multiple_of(i * tile, 128), tile)
+            both = jnp.dot(sides[: 2 * H, :], xfull[:, cols], preferred_element_type=F32)
+            out_gate[:, cols] = both[:H]
+            out_up[:, cols] = both[H:]
+            return 0
+
+        lax.fori_loop(0, D // tile, step, 0)
+
+    def weights_down():
+        def step(i, _):
+            cols = pl.ds(pl.multiple_of(i * tile, 128), tile)
+            out_down[:, cols] = jnp.dot(
+                sides[2 * H :, :], gfull[:, cols], preferred_element_type=F32
+            )
+            return 0
+
+        lax.fori_loop(0, D // tile, step, 0)
+
+    def main(i, _):
+        @pl.when(i == 0)
+        def _():
+            tokens_in(i)
+            crossed(i)
+
+        @pl.when(i == 1)
+        def _():
+            for n, (cp, src) in enumerate(zip(loads, (wg, wu, wd))):
+                cp.wait()
+                turned[n] = src[...].T
+
+        @pl.when((i >= 1) & (i < NZ))
+        def _():
+            arrivals(i)
+
+        @pl.when(i == NZ - 1)
+        def _():
+            lax.fori_loop(1, NZ, send_shared, 0)
+
+        @pl.when(i == NZ)
+        def _():
+            with jax.named_scope("share"):
+                lax.fori_loop(1, NZ, half_relay, 0)
+                combine(turn(NZ - 2))
+                lax.fori_loop(0, NZ, share, 0)
+                for d in range(1, X):
+                    sg_out[d - 1] = sg_acc[hidden_of((x + d) % X), :].astype(BF16)
+                    sg_copy(d).start()
+
+        @pl.when((i >= 1) & (i <= NZ))
+        def _():
+            with jax.named_scope("relay"):
+                relay(turn(i - 1))
+            with jax.named_scope("compute"):
+                compute(turn(i - 1))
+
+        @pl.when((i >= 1) & (i <= NZ))
+        def _():
+            with jax.named_scope("partial"):
+                spread_rows(turn(i - 1))
+
+        @pl.when(i == NZ)
+        def _():
+            for dt in range(1, T):
+                gate_tp_copy(dt).start()
+
+        @pl.when(i == NZ + 1)
+        def _():
+            with jax.named_scope("weights_up"):
+                weights_up()
+
+        @pl.when(i >= 2)
+        def _():
+            with jax.named_scope("send_back"):
+                send_back(turn(i - 2))
+
+        @pl.when((i >= 1) & (i <= NZ) & (i != NZ - 1))
+        def _():
+            with jax.named_scope("combine"):
+                combine(turn(i - 1))
+
+        return 0
+
+    lax.fori_loop(0, NZ + 2, main, 0)
 
     total = gate[...]
+    with jax.named_scope("gate_tp"):
+        for dt in range(1, T):
+            gate_tp_copy(dt).wait()
     for dt in range(1, T):
-        gate_tp_copy(dt).wait()
         total = total + gate_in[dt]
     gate_out[...] = total
     gate_back[me] = total
@@ -564,27 +687,32 @@
     others(lambda s: gate_ep_copy(s).start())
 
     value = sg_acc[hidden_of(x), :]
+    with jax.named_scope("shared_in"):
+        for d in range(1, X):
+            sg_copy(d).wait()
     for d in range(1, X):
-        sg_copy(d).wait()
         value = value + sg_in[d - 1].astype(F32)
     shared_grad[...] = value
 
+    with jax.named_scope("weights_down"):
+        weights_down()
     tg_acc[...] = jnp.zeros_like(tg_acc)
 
     def gather(j, _):
         zs = plane(j)
-        for d in range(X):
-            e = zs * X + d
-
-            @pl.when(e != me)
-            def _():
-                remote(
-                    row_out.at[rows_of(e)],
-                    back.at[rows_of(e)],
-                    back_send,
-                    back_recv.at[e],
-                    (me, tp),
-                ).wait_recv()
+        with jax.named_scope("back"):
+            for d in range(X):
+                e = zs * X + d
+
+                @pl.when(e != me)
+                def _():
+                    remote(
+                        row_out.at[rows_of(e)],
+                        back.at[rows_of(e)],
+                        back_send,
+                        back_recv.at[e],
+                        (me, tp),
+                    ).wait_recv()
 
         tg_acc[...] += lax.dot_general(
             table[group_of(zs), :], back[group_of(zs), :], TN, preferred_element_type=F32
@@ -605,7 +733,10 @@
         row = gate_back[e, pl.ds(me, 1), :]
         return values + jnp.where(routes[...] == e, row, 0.0)
 
-    gate_grad[...] = lax.fori_loop(0, E, take_gates, jnp.zeros((K, N), F32))
+    with jax.named_scope("gates"):
+        gate_grad[...] = lax.fori_loop(
+            0, E, take_gates, jnp.zeros((K, N), F32)
+        )
 
     def finish(s):
         meta_copy(s).wait_send()
@@ -613,7 +744,8 @@
         gate_ep_copy(s).wait_send()
         back_copy(s).wait_send()
 
-    others(finish)
+    with jax.named_scope("finish"):
+        others(finish)
 
     def finish_plane(j, _):
         zs = plane(j)
@@ -621,6 +753,7 @@
         @pl.when(j > 0)
         def _():
             sh_copy(zs).wait_send()
+            half_copy(zs, c).wait_send()
 
         spread_cot(zs, wait_send)
         for d in range(1, X):
@@ -692,6 +825,13 @@
         pltpu.VMEM((K, N), jnp.int32),
         pltpu.VMEM((K, N), F32),
         pltpu.VMEM((N, E * hs), BF16),
+        pltpu.VMEM((R, H), BF16),
+        pltpu.VMEM((R, H), BF16),
+        pltpu.VMEM((R, H), BF16),
+        pltpu.VMEM((3, T * F, H), BF16),
+        pltpu.VMEM((R, T * F), BF16),
+        pltpu.VMEM((R, T * F), BF16),
+        pltpu.VMEM((3 * H, R), BF16),
     ]
     sems = [
         dma((3,)),
@@ -723,24 +863,24 @@
         dma((E,)),
         dma((XO,)),
         dma((XO,)),
+        dma((NZ,)),
+        dma((NZ,)),
     ]
     return pl.pallas_call(
         functools.partial(routed_kernel, (E, T, X, C, F, N, K, H, hs)),
         out_shape=(
-            shape((R, T * F), BF16),
-            shape((R, T * F), BF16),
-            shape((R, H), BF16),
-            shape((R, H), BF16),
-            shape((R, H), BF16),
+            shape((H, T * F), F32),
+            shape((H, T * F), F32),
+            shape((H, T * F), F32),
             shape((N, F), BF16),
             shape((K, N), F32),
             shape((hs, F), F32),
         ),
         in_specs=[hbm] * 8,
-        out_specs=(vmem,) * 8,
+        out_specs=(vmem,) * 6,
         scratch_shapes=buffers + sems,
         compiler_params=pltpu.CompilerParams(
-            collective_id=0, has_side_effects=True, vmem_limit_bytes=36 * 1024 * 1024
+            collective_id=0, has_side_effects=True, vmem_limit_bytes=40 * 1024 * 1024
         ),
         name="routed",
     )(
@@ -751,94 +891,28 @@
     )
 
 
-def weights_kernel(
-    tile,
-    rows_x,
-    rows_g,
-    hidden,
-    grad_gate,
-    grad_up,
-    tokens_in,
-    shared_in,
-    gate_in,
-    out_gate,
-    out_up,
-    out_down,
-    tokens_out,
-    shared_out,
-    gate_out,
-    buf,
-    sem,
-    small_sem,
-):
-    small = (
-        pltpu.make_async_copy(tokens_in, tokens_out, small_sem.at[0]),
-        pltpu.make_async_copy(shared_in, shared_out, small_sem.at[1]),
-        pltpu.make_async_copy(gate_in, gate_out, small_sem.at[2]),
-    )
-    for cp in small:
+def store_kernel(count, *refs):
+    sems = refs[-1]
+    copies = [
+        pltpu.make_async_copy(refs[i], refs[count + i], sems.at[i]) for i in range(count)
+    ]
+    for cp in copies:
         cp.start()
-    plan = ((grad_gate, rows_x, out_gate), (grad_up, rows_x, out_up), (hidden, rows_g, out_down))
-    steps = rows_x.shape[1] // tile
-
-    def drain(i, slot, w):
-        cols = pl.ds(pl.multiple_of(i * tile, 128), tile)
-        return pltpu.make_async_copy(
-            buf.at[slot, w], plan[w][2].at[0, :, cols], sem.at[slot, w]
-        )
-
-    def step(i, _):
-        slot = i % 2
-        cols = pl.ds(pl.multiple_of(i * tile, 128), tile)
-        for w, (left, right, _) in enumerate(plan):
-
-            @pl.when(i >= 2)
-            def _():
-                drain(i - 2, slot, w).wait()
-
-            buf[slot, w] = lax.dot_general(
-                left[...], right[:, cols], TN, preferred_element_type=F32
-            )
-            drain(i, slot, w).start()
-        return 0
-
-    lax.fori_loop(0, steps, step, 0)
-    for i in range(max(steps - 2, 0), steps):
-        for w in range(3):
-            drain(i, i % 2, w).wait()
-    for cp in small:
+    for cp in copies:
         cp.wait()
 
 
-def weight_grads(
-    rows_x, rows_g, hidden, grad_gate, grad_up, tokens_grad, shared_grad, gate_grad
-):
-    H = hidden.shape[1]
-    D = rows_x.shape[1]
-    tile = 512 if D % 512 == 0 else 128
-    vmem = pl.BlockSpec(memory_space=pltpu.VMEM)
-    hbm = pl.BlockSpec(memory_space=pltpu.HBM)
-    shape = jax.ShapeDtypeStruct
+def store(*arrays):
+    count = len(arrays)
     return pl.pallas_call(
-        functools.partial(weights_kernel, tile),
-        out_shape=(
-            shape((1, H, D), F32),
-            shape((1, H, D), F32),
-            shape((1, H, D), F32),
-            shape(tokens_grad.shape, BF16),
-            shape(shared_grad.shape, F32),
-            shape(gate_grad.shape, F32),
-        ),
-        in_specs=[vmem] * 8,
-        out_specs=(hbm,) * 6,
-        scratch_shapes=[
-            pltpu.VMEM((2, 3, H, tile), F32),
-            pltpu.SemaphoreType.DMA((2, 3)),
-            pltpu.SemaphoreType.DMA((3,)),
-        ],
+        functools.partial(store_kernel, count),
+        out_shape=tuple(jax.ShapeDtypeStruct(v.shape, v.dtype) for v in arrays),
+        in_specs=[pl.BlockSpec(memory_space=pltpu.VMEM)] * count,
+        out_specs=(pl.BlockSpec(memory_space=pltpu.HBM),) * count,
+        scratch_shapes=[pltpu.SemaphoreType.DMA((count,))],
         compiler_params=pltpu.CompilerParams(vmem_limit_bytes=16 * 1024 * 1024),
-        name="weight_grads",
-    )(rows_x, rows_g, hidden, grad_gate, grad_up, tokens_grad, shared_grad, gate_grad)
+        name="store",
+    )(*arrays)
 
 
 def shards(tokens, cotangent, routes, gate_weight, w_gate, w_up, w_down, shared_hidden):
@@ -849,7 +923,7 @@
     capacity = 3 * tok_count * top_count // (2 * E)
     C = -(-capacity // 16) * 16
     hs = shared_hidden.shape[1] // E
-    rows_x, rows_g, hidden, grad_gate, grad_up, tokens_grad, gate_grad, shared_grad = routed(
+    results = routed(
         E,
         T,
         C,
@@ -865,10 +939,15 @@
         w_up,
         w_down,
     )
-    out_gate, out_up, out_down, tokens_grad, shared_grad, gate_grad = weight_grads(
-        rows_x, rows_g, hidden, grad_gate, grad_up, tokens_grad, shared_grad, gate_grad
+    out_gate, out_up, out_down, tokens_grad, gate_grad, shared_grad = store(*results)
+    return (
+        tokens_grad,
+        gate_grad.T,
+        out_gate[None],
+        out_up[None],
+        out_down[None],
+        shared_grad,
     )
-    return (tokens_grad, gate_grad.T, out_gate, out_up, out_down, shared_grad)
 
 
 def solution(mesh):

time: 98.7 us -> 84.3 us (0.85)
  Pallas kernels: 97.9 us -> 83.5 us
    pallas_call x1, Pallas kernels: 89.2 us -> 78.7 us  [routed(): pl.pallas_call(functools.partial(routed_kernel, (E, T, X, C, F, N, K, H,...]
    pallas_call x1, Pallas kernels: 8.69 us -> 4.83 us  [store(): pl.pallas_call(functools.partial(store_kernel, count), out_shape=tuple((j...]
where the time goes in v2:
time: 84.3 us; the launch traced here: 84.2 us
  Pallas kernels  83.5 us (99%)
    pallas_call x1, Pallas kernels, routed(): pl.pallas_call(functools.partial(routed_kernel, (E, T, X, C, F, N, K, H,...  78.7 us
    pallas_call x1, Pallas kernels, store(): pl.pallas_call(functools.partial(store_kernel, count), out_shape=tuple((j...  4.83 us

profile of v2, /device:TPU:0, one launch (start us, length us, event | category | flops | bytes accessed | tf_op | source)
XLA Modules:
  0.0 84.2 jit_solution(9733173371199782424)
XLA Ops:
  0.6 78.7 %routed.1 = (f32[256,4096]{1,0:T(8,128)S(1)}, f32[256,4096]{1,0:T(8,128)S(1)}, f32[256,4096]{1,0:T(8,128)S(1)}, bf16[128,1024]{1,0:T(8,128)(2,1)S(1)}, f32[2,128]{1,0:T(2,128)S(1)}, /*index=5*/f32[128,1024]{1,0:T(8,128)S(1)}) custom-call(bf16[128,1024]{1,0:T(8,128)(2,1)} %refs_0_.1, bf16[128,1024]{1,0:T(8,128)(2,1)} %refs_1_.1, s32[2,128]{1,0:T(2,128)} %bitcast.6, ...), custom_call_target="tpu_custom_call" | custom-call | tf_op jit(solution)/shard_map/routed/pallas_call | solution.py:869
  79.3 4.8 %store.1 = (f32[256,4096]{1,0:T(8,128)}, f32[256,4096]{1,0:T(8,128)}, f32[256,4096]{1,0:T(8,128)}, bf16[128,1024]{1,0:T(8,128)(2,1)}, f32[2,128]{1,0:T(2,128)}, /*index=5*/f32[128,1024]{1,0:T(8,128)}) custom-call(f32[256,4096]{1,0:T(8,128)S(1)} %get-tuple-element.18.refs_0_, f32[256,4096]{1,0:T(8,128)S(1)} %get-tuple-element.19.refs_1_, ...), custom_call_target="tpu_custom_call" | custom-call | tf_op jit(solution)/shard_map/store/pallas_call | solution.py:907

commit v3 on v2

--- a/solution.py
+++ b/solution.py
@@ -390,22 +390,35 @@
             ).wait_recv()
             forward(1, s)
 
+    edge = near == 0
+
+    def at(cond, fn, j):
+        @pl.when(cond & (j < NZ))
+        def _():
+            with jax.named_scope(fn.__name__):
+                fn(j)
+
     def arrivals(i):
-        first = (near == 0) | (i == 1)
-        second = (near >= 1) & (i + 1 < NZ)
-        for fn in (take_block, use_block, None, tokens_in, crossed):
-            if fn is None:
-                send_late(i)
-                continue
-            with jax.named_scope(fn.__name__):
-
-                @pl.when(first)
-                def _():
-                    fn(i)
-
-                @pl.when(second)
-                def _():
-                    fn(i + 1)
+        inner = near >= 1
+        pair = inner & (i == 1)
+        ahead = edge & ((i == 1) | (i == NZ - 1))
+        for fn in (take_block, use_block):
+            at(edge | pair, fn, i)
+            at(pair, fn, i + 1)
+        at(edge | pair, send_late, i)
+        at(ahead | pair, tokens_in, i)
+        at(pair, tokens_in, i + 1)
+        at(ahead | pair, crossed, i)
+        at(inner, crossed, i + 1)
+        at(inner, take_block, i + 2)
+        at(inner, use_block, i + 2)
+        at(inner & (i >= 2), send_late, i)
+        at(inner, tokens_in, i + 2)
+
+    def late_arrivals(i):
+        behind = edge & (i >= 2) & (i < NZ - 1)
+        at(behind, crossed, i)
+        at(behind, tokens_in, i)
 
     def send_shared(j, _):
         sh_copy(plane(j)).start()
@@ -424,6 +437,9 @@
                     sib_copy(a, s, dy).start()
             if d > 0:
                 meta_wait(s)
+
+    def settle(j):
+        zs = plane(j)
         for a in (0, 1):
             for dy in range(Y):
                 piece = full[a].at[group_of(zs), cols_of(((y + Y - dy) % Y) * 2 + 1 - c)]
@@ -626,35 +642,41 @@
         def _():
             lax.fori_loop(1, NZ, send_shared, 0)
 
+        @pl.when((i >= 1) & (i <= NZ))
+        def _():
+            with jax.named_scope("relay"):
+
+                @pl.when((near == 0) | (i == 1))
+                def _():
+                    relay(turn(i - 1))
+
+                settle(turn(i - 1))
+            with jax.named_scope("compute"):
+                compute(turn(i - 1))
+
+        @pl.when((i >= 1) & (i <= NZ))
+        def _():
+            with jax.named_scope("partial"):
+                spread_rows(turn(i - 1))
+
+            @pl.when((near >= 1) & (i < NZ))
+            def _():
+                with jax.named_scope("next_relay"):
+                    relay(turn(i))
+
         @pl.when(i == NZ)
         def _():
+            for dt in range(1, T):
+                gate_tp_copy(dt).start()
+            lax.fori_loop(1, NZ, half_relay, 0)
+
+        @pl.when(i == NZ + 1)
+        def _():
             with jax.named_scope("share"):
-                lax.fori_loop(1, NZ, half_relay, 0)
-                combine(turn(NZ - 2))
                 lax.fori_loop(0, NZ, share, 0)
                 for d in range(1, X):
                     sg_out[d - 1] = sg_acc[hidden_of((x + d) % X), :].astype(BF16)
                     sg_copy(d).start()
-
-        @pl.when((i >= 1) & (i <= NZ))
-        def _():
-            with jax.named_scope("relay"):
-                relay(turn(i - 1))
-            with jax.named_scope("compute"):
-                compute(turn(i - 1))
-
-        @pl.when((i >= 1) & (i <= NZ))
-        def _():
-            with jax.named_scope("partial"):
-                spread_rows(turn(i - 1))
-
-        @pl.when(i == NZ)
-        def _():
-            for dt in range(1, T):
-                gate_tp_copy(dt).start()
-
-        @pl.when(i == NZ + 1)
-        def _():
             with jax.named_scope("weights_up"):
                 weights_up()
 
@@ -663,11 +685,12 @@
             with jax.named_scope("send_back"):
                 send_back(turn(i - 2))
 
-        @pl.when((i >= 1) & (i <= NZ) & (i != NZ - 1))
+        @pl.when((i >= 1) & (i <= NZ))
         def _():
             with jax.named_scope("combine"):
                 combine(turn(i - 1))
 
+        late_arrivals(i)
         return 0
 
     lax.fori_loop(0, NZ + 2, main, 0)
@@ -685,14 +708,6 @@
         return remote(gate_out, gate_back.at[me], gate_ep_send, gate_ep_recv.at[me], (s, tp))
 
     others(lambda s: gate_ep_copy(s).start())
-
-    value = sg_acc[hidden_of(x), :]
-    with jax.named_scope("shared_in"):
-        for d in range(1, X):
-            sg_copy(d).wait()
-    for d in range(1, X):
-        value = value + sg_in[d - 1].astype(F32)
-    shared_grad[...] = value
 
     with jax.named_scope("weights_down"):
         weights_down()
@@ -737,6 +752,14 @@
         gate_grad[...] = lax.fori_loop(
             0, E, take_gates, jnp.zeros((K, N), F32)
         )
+
+    value = sg_acc[hidden_of(x), :]
+    with jax.named_scope("shared_in"):
+        for d in range(1, X):
+            sg_copy(d).wait()
+    for d in range(1, X):
+        value = value + sg_in[d - 1].astype(F32)
+    shared_grad[...] = value
 
     def finish(s):
         meta_copy(s).wait_send()

time: 84.3 us -> 79.3 us (0.941)
  Pallas kernels: 83.5 us -> 78.5 us
    pallas_call x1, Pallas kernels: 78.7 us -> 73.7 us  [routed(): pl.pallas_call(functools.partial(routed_kernel, (E, T, X, C, F, N, K, H,...]
where the time goes in v3:
time: 79.3 us; the launch traced here: 79.2 us
  Pallas kernels  78.5 us (99%)
    pallas_call x1, Pallas kernels, routed(): pl.pallas_call(functools.partial(routed_kernel, (E, T, X, C, F, N, K, H,...  73.7 us
    pallas_call x1, Pallas kernels, store(): pl.pallas_call(functools.partial(store_kernel, count), out_shape=tuple((j...  4.83 us

profile of v3, /device:TPU:0, one launch (start us, length us, event | category | flops | bytes accessed | tf_op | source)
XLA Modules:
  0.0 79.2 jit_solution(18381568005568829505)
XLA Ops:
  0.6 73.7 %routed.1 = (f32[256,4096]{1,0:T(8,128)S(1)}, f32[256,4096]{1,0:T(8,128)S(1)}, f32[256,4096]{1,0:T(8,128)S(1)}, bf16[128,1024]{1,0:T(8,128)(2,1)S(1)}, f32[2,128]{1,0:T(2,128)S(1)}, /*index=5*/f32[128,1024]{1,0:T(8,128)S(1)}) custom-call(bf16[128,1024]{1,0:T(8,128)(2,1)} %refs_0_.1, bf16[128,1024]{1,0:T(8,128)(2,1)} %refs_1_.1, s32[2,128]{1,0:T(2,128)} %bitcast.6, ...), custom_call_target="tpu_custom_call" | custom-call | tf_op jit(solution)/shard_map/routed/pallas_call | solution.py:892
  74.3 4.8 %store.1 = (f32[256,4096]{1,0:T(8,128)}, f32[256,4096]{1,0:T(8,128)}, f32[256,4096]{1,0:T(8,128)}, bf16[128,1024]{1,0:T(8,128)(2,1)}, f32[2,128]{1,0:T(2,128)}, /*index=5*/f32[128,1024]{1,0:T(8,128)}) custom-call(f32[256,4096]{1,0:T(8,128)S(1)} %get-tuple-element.18.refs_0_, f32[256,4096]{1,0:T(8,128)S(1)} %get-tuple-element.19.refs_1_, ...), custom_call_target="tpu_custom_call" | custom-call | tf_op jit(solution)/shard_map/store/pallas_call | solution.py:930
